TPU v7x, 512 devices: a whole 4x4x16 slice. The times are simulated.
512 devices in a mesh: sp: 64 (over z, y), tp: 8 (over x, core).
Axes of the slice: x: 4, y: 4, z: 16, core: 2. Of those that a mesh axis runs over, the one named last changes fastest.
Arguments:
- queries: bfloat16 [32768, 1024], P('sp', 'tp'), may hold values from -8 to 8
- key_rows: bfloat16 [32768, 512], P('sp', 'tp'), may hold values from -8 to 8
- values: bfloat16 [32768, 512], P('sp', 'tp'), may hold values from -16 to 16
- doc_ids: int32 [32768], P('sp'), may hold values from 0 to 31, never falling along the last dimension, each value on 1 to 2048 neighbouring positions
- sink_logits: float32 [16], P('tp'), may hold values from 2.5 to 6
- residual: bfloat16 [32768, 2048], P('sp'), may hold values from -6 to 6
- out_weight: bfloat16 [1024, 2048], P('tp'), may hold values from -0.1875 to 0.1875
- norm_gain: float32 [2048], replicated, may hold values from 0.1 to 1.9
- w_gate: bfloat16 [2048, 5632], P('sp', 'tp'), may hold values from -0.125 to 0.125
- w_up: bfloat16 [2048, 5632], P('sp', 'tp'), may hold values from -0.125 to 0.125
- w_down: bfloat16 [5632, 2048], P('tp', 'sp'), may hold values from -0.078125 to 0.078125
Outputs:
- layer_out: bfloat16 [32768, 2048], P('sp')
Inputs may be any that keep to these rules, and one draw needn't show every extreme that they name: `doc_ids`: document numbers never fall along the positions; each document has 1 to 2048 positions.
All inputs are finite; a program needn't handle non-finite values.
Results may differ from a plain program's by a relative error of at most 0.014.
Values may be sent and summed in bfloat16 or wider, within the bound.
No kernel may reach another device: no remote copies, remote signals or barrier semaphores. Data moves between devices by JAX's collectives and lax.ppermute only.
A program may use at most 64 MiB of HBM per device.

v0:
```python
import jax
import jax.numpy as jnp
from jax import lax
from jax.sharding import PartitionSpec as P

HD = 64
WINDOW = 128


def from_behind(shard, axis, by):
    size = lax.axis_size(axis)
    pairs = [(i, i + by) for i in range(size) if 0 <= i + by < size]
    return lax.ppermute(shard, axis, pairs)


def gather_turned(arrays, axis, dims):
    turned = [jnp.moveaxis(a, dim, 0) for a, dim in zip(arrays, dims)]
    both = jnp.concatenate([t.reshape(len(t), -1) for t in turned], axis=1)
    result, at, finished = (lax.all_gather(both, axis, axis=0, tiled=True), 0, [])
    for t, dim in zip(turned, dims):
        slab = result[:, at : at + t[0].size].reshape(-1, *t.shape[1:])
        finished.append(jnp.moveaxis(slab, 0, dim))
        at += t[0].size
    return tuple(finished)


def cut_along(shard, dim, size):
    before, after = (shard.shape[:dim], shard.shape[dim + 1 :])
    return jnp.moveaxis(shard.reshape(*before, size, -1, *after), dim, 0)


def sum_at_owner(shard, axis, dim):
    pieces = cut_along(shard, dim, lax.axis_size(axis))
    arrived = lax.all_to_all(pieces, axis, split_axis=0, concat_axis=0, tiled=True)
    return arrived.astype(jnp.float32).sum(axis=0)


def laid_out(pieces, dim):
    dims = list(pieces.shape[1:])
    dims[dim] *= pieces.shape[0]
    return jnp.moveaxis(pieces, 0, dim).reshape(dims)


def sent_to_all(shard, axis):
    size = lax.axis_size(axis)
    return lax.all_to_all(
        jnp.broadcast_to(shard[None], (size, *shard.shape)), axis, 0, 0, tiled=True
    )


def gathered_copies(shard, axis, dim):
    return laid_out(sent_to_all(shard, axis), dim)


def rms_norm(stream, norm_gain):
    floats = stream.astype(jnp.float32)
    scale = lax.rsqrt(jnp.mean(floats * floats, axis=-1, keepdims=True) + 1e-06)
    return floats * scale * norm_gain


def band_rows(tensor, blocks):
    tensor = tensor.reshape((blocks + 1, WINDOW) + tensor.shape[1:])
    return jnp.concatenate([tensor[:-1], tensor[1:]], axis=1)


def attend(queries, key_rows, values, doc_ids, sink_logits):
    local_rows = queries.shape[0]
    blocks = local_rows // WINDOW
    kv_local = key_rows.shape[1] // HD
    per_kv = queries.shape[1] // key_rows.shape[1]
    tail_docs = doc_ids[local_rows - WINDOW :] + 1
    prev_keys, prev_values, prev_docs = from_behind(
        (key_rows[local_rows - WINDOW :], values[local_rows - WINDOW :], tail_docs), "sp", 1
    )
    key_band = band_rows(jnp.concatenate([prev_keys, key_rows], axis=0), blocks).reshape(
        blocks, 2 * WINDOW, kv_local, HD
    )
    value_band = band_rows(jnp.concatenate([prev_values, values], axis=0), blocks).reshape(
        blocks, 2 * WINDOW, kv_local, HD
    )
    doc_band = band_rows(jnp.concatenate([prev_docs - 1, doc_ids]), blocks)
    query_band = queries.reshape(blocks, WINDOW, kv_local, per_kv, HD)
    scores = jnp.einsum(
        "nqhgd,nkhd->nhgqk", query_band, key_band, preferred_element_type=jnp.float32
    ) * HD ** (-0.5)
    offsets = jnp.arange(WINDOW)[:, None] + WINDOW - jnp.arange(2 * WINDOW)[None, :]
    inside = (offsets >= 0) & (offsets < WINDOW)
    query_docs = doc_ids.reshape(blocks, WINDOW)
    allowed = inside[None] & (query_docs[:, :, None] == doc_band[:, None, :])
    scores = jnp.where(allowed[:, None, None], scores, -1e30)
    sink_logit = sink_logits.reshape(kv_local, per_kv)[None, :, :, None, None]
    peak = jnp.maximum(jnp.max(scores, axis=-1, keepdims=True), sink_logit)
    raised = jnp.exp(scores - peak)
    denom = jnp.sum(raised, axis=-1, keepdims=True) + jnp.exp(sink_logit - peak)
    weights = (raised / denom).astype(jnp.bfloat16)
    attended = jnp.einsum(
        "nhgqk,nkhd->nqhgd", weights, value_band, preferred_element_type=jnp.float32
    )
    return attended.astype(jnp.bfloat16).reshape(local_rows, queries.shape[1])


def on_device(
    queries,
    key_rows,
    values,
    doc_ids,
    sink_logits,
    residual,
    out_weight,
    norm_gain,
    w_gate,
    w_up,
    w_down,
):
    gate_whole, up_whole, down_whole = gather_turned((w_gate, w_up, w_down), "sp", (0, 0, 1))
    attended = attend(queries, key_rows, values, doc_ids, sink_logits)
    row_share = residual.shape[0] // lax.axis_size("tp")
    picked = attended
    mixed_sum = sum_at_owner(
        jnp.dot(picked, out_weight, preferred_element_type=jnp.float32).astype(jnp.bfloat16),
        "tp",
        0,
    )
    base_rows = lax.dynamic_slice_in_dim(residual, lax.axis_index("tp") * row_share, row_share, 0)
    stream = (base_rows.astype(jnp.float32) + mixed_sum).astype(jnp.bfloat16)
    normed = rms_norm(stream, norm_gain).astype(jnp.bfloat16)
    normed = gathered_copies(normed, "tp", 0)
    gate_act = jnp.dot(normed, gate_whole, preferred_element_type=jnp.float32)
    up_act = jnp.dot(normed, up_whole, preferred_element_type=jnp.float32)
    hidden = (jax.nn.silu(gate_act) * up_act).astype(jnp.bfloat16)
    picked = hidden
    mlp_total = sum_at_owner(
        jnp.dot(picked, down_whole, preferred_element_type=jnp.float32).astype(jnp.bfloat16),
        "tp",
        0,
    )
    finished = (stream.astype(jnp.float32) + mlp_total).astype(jnp.bfloat16)
    return gathered_copies(finished, "tp", 0)


def solution(mesh):
    in_specs = (
        P("sp", "tp"),
        P("sp", "tp"),
        P("sp", "tp"),
        P("sp"),
        P("tp"),
        P("sp", None),
        P("tp", None),
        P(),
        P("sp", "tp"),
        P("sp", "tp"),
        P("tp", "sp"),
    )
    out_specs = P("sp", None)
    return jax.shard_map(
        on_device, mesh=mesh, in_specs=in_specs, out_specs=out_specs, check_vma=False
    )
```

profile of v0, /device:TPU:1, one launch (start us, length us, event | category | flops | bytes accessed | tf_op | source)
XLA Modules:
  0.0 256.9 jit_solution(4028181509367564481)
XLA Ops:
  6.5 1.7 concatenate.27
  8.9 4.0 %collective-permute-start.1 = (s32[128]{0:T(128)S(1)}, s32[128]{0:T(128)S(1)}, u32[]{:S(2)}, u32[]{:S(2)}) collective-permute-start(s32[128]{0:T(128)S(1)} %slice_add_fusion), channel_id=1, source_target_pairs={{0,8},{8,16},{16,24},{24,32},{32,40},{40,48},{48,56},{56,64},{64,7... | collective-permute-start | bytes 1544 | tf_op jit(solution)/shard_map/ppermute | solution.py:13
  12.9 0.7 slice.56
  13.7 3.2 %collective-permute-start = (bf16[128,64]{0,1:T(8,128)(2,1)S(1)}, bf16[128,64]{0,1:T(8,128)(2,1)S(1)}, u32[]{:S(2)}, u32[]{:S(2)}) collective-permute-start(bf16[128,64]{0,1:T(8,128)(2,1)S(1)} %slice.56), channel_id=1, source_target_pairs={{0,8},{8,16},{16,24},{24,32},{32,40},{40,48},{48,56},{56,64},{64,7... | collective-permute-start | bytes 49160 | tf_op jit(solution)/shard_map/ppermute | solution.py:13
  16.9 0.7 slice.63
  17.6 2.9 %collective-permute-start.2 = (bf16[128,64]{0,1:T(8,128)(2,1)S(1)}, bf16[128,64]{0,1:T(8,128)(2,1)S(1)}, u32[]{:S(2)}, u32[]{:S(2)}) collective-permute-start(bf16[128,64]{0,1:T(8,128)(2,1)S(1)} %slice.63), channel_id=1, source_target_pairs={{0,8},{8,16},{16,24},{24,32},{32,40},{40,48},{48,56},{56,64},{64,7... | collective-permute-start | bytes 49160 | tf_op jit(solution)/shard_map/ppermute | solution.py:13
  20.5 0.9 copy_bitcast_fusion
  21.4 0.9 copy_bitcast_fusion.2
  22.3 1.0 reshape.134
  23.3 0.7 pad_add_fusion
  24.7 0.9 compare_and_fusion
  25.6 0.8 copy_bitcast_fusion.1
  26.4 0.8 copy_bitcast_fusion.3
  28.4 2.1 convolution_convert_fusion
  30.4 5.8 %all-to-all-start = ((bf16[8,64,2048]{2,1,0:T(8,128)(2,1)}), bf16[8,64,2048]{2,1,0:T(8,128)(2,1)S(1)}, u32[]{:S(2)}, u32[]{:S(2)}) async-start(bf16[8,64,2048]{2,1,0:T(8,128)(2,1)} %bitcast.63), calls=%async_computation | async-start | bytes 4194304 | tf_op jit(solution)/shard_map/all_to_all | solution.py:34
  36.2 26.2 %all-to-all-done = bf16[8,64,2048]{2,1,0:T(8,128)(2,1)S(1)} async-done(((bf16[8,64,2048]{2,1,0:T(8,128)(2,1)}), bf16[8,64,2048]{2,1,0:T(8,128)(2,1)S(1)}, u32[]{:S(2)}, u32[]{:S(2)}) %all-to-all-start) | async-done | bytes 2097184 | tf_op jit(solution)/shard_map/all_to_all | solution.py:34
  62.8 1.1 fusion.22
  64.4 29.6 %all_to_all.20 = bf16[8,64,2048]{2,1,0:T(8,128)(2,1)S(1)} all-to-all(bf16[8,64,2048]{2,1,0:T(8,128)(2,1)S(1)} %broadcast_in_dim.18), channel_id=1, replica_groups=mesh['sp'=64,'tp'=8] {'tp'}, dimensions={0} | all-to-all | bytes 4194304 | tf_op jit(solution)/shard_map/all_to_all | solution.py:46
  94.0 71.6 %all-gather.2.cloned.1.call-done = bf16[2048,2112]{1,0:T(8,128)(2,1)} async-done(((bf16[32,2112]{1,0:T(8,128)(2,1)}), bf16[2048,2112]{1,0:T(8,128)(2,1)}) %all-gather.2.cloned.1.call-update) | async-done | bytes 8650768 | tf_op jit(solution)/shard_map/all_gather | solution.py:19
  165.5 4.7 %fusion.4 = f32[512,704]{0,1:T(8,128)} fusion(bf16[512,2048]{1,0:T(8,128)(2,1)S(1)} %bitcast.65, bf16[2048,2112]{1,0:T(8,128)(2,1)} %all-gather.2.cloned.1.call-done), kind=kOutput, calls=%fused_computation.6 | convolution fusion | flops 1476395008 | bytes 6684672 | tf_op jit(solution)/shard_map/dot_general | solution.py:128
  170.3 9.4 %fusion.6 = bf16[512,2048]{1,0:T(8,128)(2,1)} fusion(bf16[2048,2112]{1,0:T(8,128)(2,1)} %all-gather.2.cloned.1.call-done, bf16[512,2048]{1,0:T(8,128)(2,1)S(1)} %bitcast.66, f32[512,704]{0,1:T(8,128)} %fusion.4), kind=kOutput, calls=%fused_computation.9 | convolution fusion | flops 2956001280 | bytes 11927552 | tf_op jit(solution)/shard_map/dot_general | solution.py:133
  179.7 38.7 %all_to_all.21 = bf16[8,64,2048]{2,1,0:T(8,128)(2,1)S(1)} all-to-all(bf16[8,64,2048]{2,1,0:T(8,128)(2,1)} %bitcast.67), channel_id=1, replica_groups=mesh['sp'=64,'tp'=8] {'tp'}, dimensions={0} | all-to-all | bytes 4194304 | tf_op jit(solution)/shard_map/all_to_all | solution.py:34
  219.1 29.7 %all_to_all.22 = bf16[8,64,2048]{2,1,0:T(8,128)(2,1)S(1)} all-to-all(bf16[8,64,2048]{2,1,0:T(8,128)(2,1)S(1)} %broadcast_in_dim.19), channel_id=1, replica_groups=mesh['sp'=64,'tp'=8] {'tp'}, dimensions={0} | all-to-all | bytes 4194304 | tf_op jit(solution)/shard_map/all_to_all | solution.py:46
  248.7 1.3 copy.45
  (30 shorter events, 4.0 us)
Async XLA Ops:
  6.5 21.8 %copy-start = (bf16[128,2048]{1,0:T(8,128)(2,1)S(1)}, bf16[128,2048]{1,0:T(8,128)(2,1)}, u32[]{:S(2)}) copy-start(bf16[128,2048]{1,0:T(8,128)(2,1)} %param.17) | copy-start | bytes 1572868
  6.5 21.1 %copy-start.2 = (f32[2]{0:T(128)S(1)}, f32[2]{0:T(128)}, u32[]{:S(2)}) copy-start(f32[2]{0:T(128)} %param.15) | copy-start | bytes 28
  6.5 159.0 %all-gather.2.cloned.1.call-start = ((), (), s32[]{:S(2)}) async-start(), calls=%async_computation.4 | async-start | bytes 9052160 | tf_op jit(solution)/shard_map/all_gather | solution.py:19
  8.9 14.4 %collective-permute-start.1 = (s32[128]{0:T(128)S(1)}, s32[128]{0:T(128)S(1)}, u32[]{:S(2)}, u32[]{:S(2)}) collective-permute-start(s32[128]{0:T(128)S(1)} %slice_add_fusion), channel_id=1, source_target_pairs={{0,8},{8,16},{16,24},{24,32},{32,40},{40,48},{48,56},{56,64},{64,7... | collective-permute-start | bytes 1544 | tf_op jit(solution)/shard_map/ppermute | solution.py:13
  13.7 12.8 %collective-permute-start = (bf16[128,64]{0,1:T(8,128)(2,1)S(1)}, bf16[128,64]{0,1:T(8,128)(2,1)S(1)}, u32[]{:S(2)}, u32[]{:S(2)}) collective-permute-start(bf16[128,64]{0,1:T(8,128)(2,1)S(1)} %slice.56), channel_id=1, source_target_pairs={{0,8},{8,16},{16,24},{24,32},{32,40},{40,48},{48,56},{56,64},{64,7... | collective-permute-start | bytes 49160 | tf_op jit(solution)/shard_map/ppermute | solution.py:13
  17.6 8.0 %collective-permute-start.2 = (bf16[128,64]{0,1:T(8,128)(2,1)S(1)}, bf16[128,64]{0,1:T(8,128)(2,1)S(1)}, u32[]{:S(2)}, u32[]{:S(2)}) collective-permute-start(bf16[128,64]{0,1:T(8,128)(2,1)S(1)} %slice.63), channel_id=1, source_target_pairs={{0,8},{8,16},{16,24},{24,32},{32,40},{40,48},{48,56},{56,64},{64,7... | collective-permute-start | bytes 49160 | tf_op jit(solution)/shard_map/ppermute | solution.py:13
  30.4 32.0 %all-to-all-start = ((bf16[8,64,2048]{2,1,0:T(8,128)(2,1)}), bf16[8,64,2048]{2,1,0:T(8,128)(2,1)S(1)}, u32[]{:S(2)}, u32[]{:S(2)}) async-start(bf16[8,64,2048]{2,1,0:T(8,128)(2,1)} %bitcast.63), calls=%async_computation | async-start | bytes 4194304 | tf_op jit(solution)/shard_map/all_to_all | solution.py:34
  36.2 27.7 %copy-start.1 = (f32[2048]{0:T(1024)S(1)}, f32[2048]{0:T(1024)}, u32[]{:S(2)}) copy-start(f32[2048]{0:T(1024)} %param.18) | copy-start | bytes 24580
Sparse Core Ops, SparseCore 0:
  10.3 155.2 all-gather.1
where the time goes:
time: 258 us; the launch traced here: 257 us
  blocking collectives  97.9 us (38%)
  waiting for transfers between devices  97.8 us (38%)
  matrix products  16.9 us (7%)
  starting transfers between devices  15.9 us (6%)
  between operations  13.6 us (5%)
  local copies, waits for them, and re-layouts  7.79 us (3%)
  other arithmetic  6.98 us (3%)
    all_gather x1, waiting for transfers between devices, gather_turned(): lax.all_gather(both, axis, axis=0, tiled=True)  71.6 us
    all_to_all x2, blocking collectives, sent_to_all(): lax.all_to_all(jnp.broadcast_to(shard[None], (size, *shard.shape)), axis,...  59.2 us
    all_to_all x1, blocking collectives, sum_at_owner(): lax.all_to_all(pieces, axis, split_axis=0, concat_axis=0, tiled=True)  38.7 us
    all_to_all x1, waiting for transfers between devices, sum_at_owner(): lax.all_to_all(pieces, axis, split_axis=0, concat_axis=0, tiled=True)  26.2 us
    ppermute x3, starting transfers between devices, from_behind(): return lax.ppermute(shard, axis, pairs)  10.1 us
    dot_general x1, matrix products, on_device(): jnp.dot(picked, down_whole, preferred_element_type=jnp.float32)  9.43 us
    all_to_all x1, starting transfers between devices, sum_at_owner(): lax.all_to_all(pieces, axis, split_axis=0, concat_axis=0, tiled=True)  5.81 us
  transfers between devices with their start and end apart: 5, of which 2 were waited for; matrix products, arithmetic and copies ran while one was open for 5% of the time, Pallas kernels for 0%

commit v1 on v0

--- a/solution.py
+++ b/solution.py
@@ -2,9 +2,18 @@
 import jax.numpy as jnp
 from jax import lax
 from jax.sharding import PartitionSpec as P
+from jax.lax import all_to_all, axis_size
 
 HD = 64
 WINDOW = 128
+
+
+def digits_advance(original, group_axis):
+    far_arr = jnp.stack(axis_size(group_axis) * [original], axis=0)
+    part_now = jnp.concatenate(
+        all_to_all(far_arr, axis_name=group_axis, split_axis=0, concat_axis=0), 0
+    )
+    return part_now
 
 
 def from_behind(shard, axis, by):
@@ -16,7 +25,7 @@
 def gather_turned(arrays, axis, dims):
     turned = [jnp.moveaxis(a, dim, 0) for a, dim in zip(arrays, dims)]
     both = jnp.concatenate([t.reshape(len(t), -1) for t in turned], axis=1)
-    result, at, finished = (lax.all_gather(both, axis, axis=0, tiled=True), 0, [])
+    result, at, finished = (digits_advance(both, group_axis=axis), 0, [])
     for t, dim in zip(turned, dims):
         slab = result[:, at : at + t[0].size].reshape(-1, *t.shape[1:])
         finished.append(jnp.moveaxis(slab, 0, dim))

time: 258 us -> 577 us (2.24)
  blocking collectives: 97.9 us -> 470 us
  waiting for transfers between devices: 97.8 us -> 52.3 us
  between operations: 13.6 us -> 0.22 us
    all_to_all x0 -> x1, blocking collectives: none -> 407 us  [digits_advance(): all_to_all(far_arr, axis_name=group_axis, split_axis=0, concat_axis=0)]
    all_gather x1 -> x0, waiting for transfers between devices: 71.6 us -> none  [gather_turned(): lax.all_gather(both, axis, axis=0, tiled=True)]
    all_to_all x2 -> x1, blocking collectives: 59.2 us -> 29.7 us  [sent_to_all(): lax.all_to_all(jnp.broadcast_to(shard[None], (size, *shard.shape)), axis,...]
    all_to_all x0 -> x1, waiting for transfers between devices: none -> 26.1 us  [sent_to_all(): lax.all_to_all(jnp.broadcast_to(shard[None], (size, *shard.shape)), axis,...]
  transfers between devices with their start and end apart: 5 -> 5, of which waited for: 2 -> 2; matrix products, arithmetic and copies ran while one was open for 5% -> 1% of each run, Pallas kernels for 0% -> 0%
where the time goes in v1:
time: 577 us; the launch traced here: 576 us
  blocking collectives  470 us (81%)
  waiting for transfers between devices  52.3 us (9%)
  starting transfers between devices  20.5 us (4%)
  matrix products  15 us (3%)
  local copies, waits for them, and re-layouts  11.7 us (2%)
  other arithmetic  6.18 us (1%)
    all_to_all x1, blocking collectives, digits_advance(): all_to_all(far_arr, axis_name=group_axis, split_axis=0, concat_axis=0)  407 us
    all_to_all x1, blocking collectives, sum_at_owner(): lax.all_to_all(pieces, axis, split_axis=0, concat_axis=0, tiled=True)  33.7 us
    all_to_all x1, blocking collectives, sent_to_all(): lax.all_to_all(jnp.broadcast_to(shard[None], (size, *shard.shape)), axis,...  29.7 us
    all_to_all x1, waiting for transfers between devices, sum_at_owner(): lax.all_to_all(pieces, axis, split_axis=0, concat_axis=0, tiled=True)  26.2 us
    all_to_all x1, waiting for transfers between devices, sent_to_all(): lax.all_to_all(jnp.broadcast_to(shard[None], (size, *shard.shape)), axis,...  26.1 us
  transfers between devices with their start and end apart: 5, of which 2 were waited for; matrix products, arithmetic and copies ran while one was open for 1% of the time, Pallas kernels for 0%

profile of v1, /device:TPU:1, one launch (start us, length us, event | category | flops | bytes accessed | tf_op | source)
XLA Modules:
  0.0 576.0 jit_solution(7722270333320070947)
XLA Ops:
  0.0 0.8 slice.63
  0.8 4.0 collective-permute-start.2
  5.5 3.2 collective-permute-start.1
  8.7 0.7 slice.56
  9.4 2.9 collective-permute-start
  12.3 0.9 copy_bitcast_fusion
  13.2 0.9 copy_bitcast_fusion.2
  14.1 1.0 reshape.140
  16.6 0.9 compare_and_fusion
  17.5 0.8 copy_bitcast_fusion.1
  19.4 2.0 convolution_convert_fusion
  21.5 5.8 %all-to-all-start = ((bf16[8,64,2048]{2,1,0:T(8,128)(2,1)}), bf16[8,64,2048]{2,1,0:T(8,128)(2,1)S(1)}, u32[]{:S(2)}, u32[]{:S(2)}) async-start(bf16[8,64,2048]{2,1,0:T(8,128)(2,1)} %bitcast.66), calls=%async_computation | async-start | bytes 4194304 | tf_op jit(solution)/shard_map/all_to_all | solution.py:43
  27.3 26.2 %all-to-all-done = bf16[8,64,2048]{2,1,0:T(8,128)(2,1)S(1)} async-done(((bf16[8,64,2048]{2,1,0:T(8,128)(2,1)}), bf16[8,64,2048]{2,1,0:T(8,128)(2,1)S(1)}, u32[]{:S(2)}, u32[]{:S(2)}) %all-to-all-start) | async-done | bytes 2097184 | tf_op jit(solution)/shard_map/all_to_all | solution.py:43
  53.9 1.1 fusion.22
  55.2 1.6 broadcast_in_dim.18
  56.8 4.6 all-to-all-start.1
  61.5 26.1 %all-to-all-done.1 = bf16[8,64,2048]{2,1,0:T(8,128)(2,1)S(1)} async-done(((bf16[8,64,2048]{2,1,0:T(8,128)(2,1)}), bf16[8,64,2048]{2,1,0:T(8,128)(2,1)S(1)}, u32[]{:S(2)}, u32[]{:S(2)}) %all-to-all-start.1) | async-done | bytes 2097184 | tf_op jit(solution)/shard_map/all_to_all | solution.py:55
  88.2 406.7 %all_to_all.25 = bf16[64,32,2112]{2,1,0:T(8,128)(2,1)S(1)} all-to-all(bf16[64,32,2112]{2,1,0:T(8,128)(2,1)S(1)} %stack.2), channel_id=1, replica_groups=mesh['sp'=64,'tp'=8] {'sp'}, dimensions={0} | all-to-all | bytes 17301504 | tf_op jit(solution)/shard_map/all_to_all | solution.py:14
  494.9 3.4 copy-done.1
  498.3 2.8 fusion.4
  501.2 9.4 %fusion.6 = bf16[512,2048]{1,0:T(8,128)(2,1)} fusion(bf16[2048,2112]{1,0:T(8,128)(2,1)} %bitcast.65, bf16[512,2048]{1,0:T(8,128)(2,1)S(1)} %bitcast.69, f32[512,704]{0,1:T(8,128)} %fusion.4), kind=kOutput, calls=%fused_computation.9 | convolution fusion | flops 2956001280 | bytes 11927552 | tf_op jit(solution)/shard_map/dot_general | solution.py:142
  510.6 33.7 %all_to_all.26 = bf16[8,64,2048]{2,1,0:T(8,128)(2,1)S(1)} all-to-all(bf16[8,64,2048]{2,1,0:T(8,128)(2,1)} %bitcast.70), channel_id=1, replica_groups=mesh['sp'=64,'tp'=8] {'tp'}, dimensions={0} | all-to-all | bytes 4194304 | tf_op jit(solution)/shard_map/all_to_all | solution.py:43
  545.0 29.7 %all_to_all.27 = bf16[8,64,2048]{2,1,0:T(8,128)(2,1)S(1)} all-to-all(bf16[8,64,2048]{2,1,0:T(8,128)(2,1)S(1)} %broadcast_in_dim.19), channel_id=1, replica_groups=mesh['sp'=64,'tp'=8] {'tp'}, dimensions={0} | all-to-all | bytes 4194304 | tf_op jit(solution)/shard_map/all_to_all | solution.py:55
  574.7 1.3 copy.45
  (40 shorter events, 5.1 us)
Async XLA Ops:
  0.0 19.4 %copy-start = (bf16[128,2048]{1,0:T(8,128)(2,1)S(1)}, bf16[128,2048]{1,0:T(8,128)(2,1)}, u32[]{:S(2)}) copy-start(bf16[128,2048]{1,0:T(8,128)(2,1)} %param.17) | copy-start | bytes 1572868
  0.0 19.0 %copy-start.2 = (bf16[512,64]{0,1:T(8,128)(2,1)S(1)}, bf16[512,64]{0,1:T(8,128)(2,1)}, u32[]{:S(2)}) copy-start(bf16[512,64]{0,1:T(8,128)(2,1)} %param.13) | copy-start | bytes 196612
  0.0 18.6 %copy-start.7 = (f32[2]{0:T(128)S(1)}, f32[2]{0:T(128)}, u32[]{:S(2)}) copy-start(f32[2]{0:T(128)} %param.15) | copy-start | bytes 28
  0.8 16.6 %collective-permute-start.2 = (bf16[128,64]{0,1:T(8,128)(2,1)S(1)}, bf16[128,64]{0,1:T(8,128)(2,1)S(1)}, u32[]{:S(2)}, u32[]{:S(2)}) collective-permute-start(bf16[128,64]{0,1:T(8,128)(2,1)S(1)} %slice.63), channel_id=1, source_target_pairs={{0,8},{8,16},{16,24},{24,32},{32,40},{40,48},{48,56},{56,64},{64,7... | collective-permute-start | bytes 49160 | tf_op jit(solution)/shard_map/ppermute | solution.py:22
  5.5 9.7 %collective-permute-start.1 = (s32[128]{0:T(128)S(1)}, s32[128]{0:T(128)S(1)}, u32[]{:S(2)}, u32[]{:S(2)}) collective-permute-start(s32[128]{0:T(128)S(1)} %slice_add_fusion), channel_id=1, source_target_pairs={{0,8},{8,16},{16,24},{24,32},{32,40},{40,48},{48,56},{56,64},{64,7... | collective-permute-start | bytes 1544 | tf_op jit(solution)/shard_map/ppermute | solution.py:22
  9.4 9.5 %collective-permute-start = (bf16[128,64]{0,1:T(8,128)(2,1)S(1)}, bf16[128,64]{0,1:T(8,128)(2,1)S(1)}, u32[]{:S(2)}, u32[]{:S(2)}) collective-permute-start(bf16[128,64]{0,1:T(8,128)(2,1)S(1)} %slice.56), channel_id=1, source_target_pairs={{0,8},{8,16},{16,24},{24,32},{32,40},{40,48},{48,56},{56,64},{64,7... | collective-permute-start | bytes 49160 | tf_op jit(solution)/shard_map/ppermute | solution.py:22
  21.5 32.0 %all-to-all-start = ((bf16[8,64,2048]{2,1,0:T(8,128)(2,1)}), bf16[8,64,2048]{2,1,0:T(8,128)(2,1)S(1)}, u32[]{:S(2)}, u32[]{:S(2)}) async-start(bf16[8,64,2048]{2,1,0:T(8,128)(2,1)} %bitcast.66), calls=%async_computation | async-start | bytes 4194304 | tf_op jit(solution)/shard_map/all_to_all | solution.py:43
  27.3 27.7 %copy-start.6 = (f32[2048]{0:T(1024)S(1)}, f32[2048]{0:T(1024)}, u32[]{:S(2)}) copy-start(f32[2048]{0:T(1024)} %param.18) | copy-start | bytes 24580
  56.7 4.6 copy-start.3
  56.7 4.6 copy-start.4
  56.7 4.6 copy-start.5
  56.8 30.8 %all-to-all-start.1 = ((bf16[8,64,2048]{2,1,0:T(8,128)(2,1)}), bf16[8,64,2048]{2,1,0:T(8,128)(2,1)S(1)}, u32[]{:S(2)}, u32[]{:S(2)}) async-start(bf16[8,64,2048]{2,1,0:T(8,128)(2,1)} %broadcast_in_dim.18), calls=%async_computation.1 | async-start | bytes 4194304 | tf_op jit(solution)/shard_map/all_to_all | solution.py:55
  494.9 3.4 copy-start.1
